TPU v7x, 32 devices: a whole 2x2x4 slice. The times are simulated.
32 devices in a mesh: ep: 8 (over z, core), tp: 4 (over y, x).
Axes of the slice: x: 2, y: 2, z: 4, core: 2. Of those that a mesh axis runs over, the one named last changes fastest.
Arguments:
- hidden: bfloat16 [96, 2048], P('ep'), may hold values from -6 to 6
- pre_gain: bfloat16 [2048], replicated, may hold values from 0.099609375 to 1.8984375
- query_weight: bfloat16 [2048, 1024], P('ep', 'tp'), may hold values from -0.125 to 0.125
- key_cache: bfloat16 [96, 1024, 1024], P('ep', 'tp'), may hold values from -6 to 6
- value_cache: bfloat16 [96, 1024, 1024], P('ep', 'tp'), may hold values from -6 to 6
- lengths: int32 [96], P('ep'), may hold values from 128 to 1024
- stick_bias: float32 [16], P('tp'), may hold values from -8.5 to -3
- out_weight: bfloat16 [1024, 2048], P('tp', 'ep'), may hold values from -0.1875 to 0.1875
- post_gain: bfloat16 [2048], replicated, may hold values from 0.099609375 to 1.8984375
- ffn_gain: bfloat16 [2048], replicated, may hold values from 0.099609375 to 1.8984375
- expert_ids: int32 [96, 2], P('ep'), may hold values from 0 to 7, as said below
- route_logits: float32 [96, 2], P('ep'), may hold values from -6 to 6
- gate_experts: bfloat16 [8, 2048, 2048], P('ep', None, 'tp'), may hold values from -0.125 to 0.125
- up_experts: bfloat16 [8, 2048, 2048], P('ep', None, 'tp'), may hold values from -0.125 to 0.125
- down_experts: bfloat16 [8, 2048, 2048], P('ep', 'tp'), may hold values from -2 to 2
- out_gain: bfloat16 [2048], P('tp'), may hold values from 0.099609375 to 1.8984375
Outputs:
- result: bfloat16 [96, 2048], P('ep', 'tp')
Inputs may be any that keep to these rules, and one draw needn't show every extreme that they name: `expert_ids`: each row names 2 different experts of one group of 4 consecutive experts. Among the rows of one device (aligned blocks of 12 rows) no expert is named more than 6 times, and one expert is named exactly 6 times in every block.
All inputs are finite; a program needn't handle non-finite values.
Results may differ from a plain program's by a relative error of at most 0.014.
Values may be sent and summed in bfloat16 or wider, within the bound.
No kernel may reach another device: no remote copies, remote signals or barrier semaphores. Data moves between devices by JAX's collectives and lax.ppermute only.
A program may use at most 64 MiB of HBM per device.

v0:
```python
import jax
import jax.numpy as jnp
from jax import lax
from jax.sharding import PartitionSpec as P

epsilon = 1e-06


def inverse_rms(squares, features):
    return lax.rsqrt(squares / features + epsilon)


def stick_read(queries, key_blocks, value_blocks, lengths, head_bias):
    sequences, heads, head_size = queries.shape
    positions = key_blocks.shape[3]
    scores = jnp.einsum("she,shec->shc", queries, key_blocks, preferred_element_type=jnp.float32)
    scores = scores * head_size ** (-0.5) + head_bias[None, :, None]
    places = lax.broadcasted_iota(jnp.int32, (sequences, heads, positions), 2)
    inside = places < lengths[:, None, None]
    log_fail = jnp.where(inside, jax.nn.log_sigmoid(-scores), 0.0)
    after_sum = lax.cumsum(log_fail, axis=2, reverse=True) - log_fail
    weight = jnp.where(inside, jnp.exp(jax.nn.log_sigmoid(scores) + after_sum), 0.0).astype(
        jnp.bfloat16
    )
    mixed_heads = jnp.einsum(
        "shc,shec->she", weight, value_blocks, preferred_element_type=jnp.float32
    )
    return mixed_heads.astype(jnp.bfloat16)


def per_device(
    hidden,
    pre_gain,
    query_weight,
    key_cache,
    value_cache,
    lengths,
    stick_bias,
    out_weight,
    post_gain,
    ffn_gain,
    expert_ids,
    route_logits,
    gate_experts,
    up_experts,
    down_experts,
    out_gain,
):
    sequences, features = hidden.shape
    ep_count = lax.axis_size("ep")
    tp_count = lax.axis_size("tp")
    tp_place = lax.axis_index("tp")
    heads_here = stick_bias.shape[0]
    head_size = key_cache.shape[1] // heads_here
    positions = key_cache.shape[2]
    slice_width = features // tp_count
    hidden_wide = hidden.astype(jnp.float32)
    normed = (
        hidden_wide
        * inverse_rms(jnp.sum(hidden_wide * hidden_wide, axis=1, keepdims=True), features)
        * pre_gain.astype(jnp.float32)
    ).astype(jnp.bfloat16)
    queries = jnp.dot(
        normed,
        lax.all_gather(query_weight, "ep", axis=0, tiled=True),
        preferred_element_type=jnp.float32,
    )
    queries = queries.astype(jnp.bfloat16).reshape(sequences, heads_here, head_size)
    key_blocks = key_cache.reshape(sequences, heads_here, head_size, positions)
    value_blocks = value_cache.reshape(sequences, heads_here, head_size, positions)
    mixed_heads = stick_read(queries, key_blocks, value_blocks, lengths, stick_bias)
    mixed_heads = mixed_heads.reshape(sequences, heads_here * head_size)
    partial_value = jnp.dot(
        mixed_heads,
        lax.all_gather(out_weight, "ep", axis=1, tiled=True),
        preferred_element_type=jnp.float32,
    )
    attended = lax.psum(partial_value, "tp").astype(jnp.bfloat16)
    attended = lax.optimization_barrier(attended).astype(jnp.float32)
    residual = (
        hidden_wide
        + attended
        * inverse_rms(jnp.sum(attended * attended, axis=1, keepdims=True), features)
        * post_gain.astype(jnp.float32)
    ).astype(jnp.bfloat16)
    residual_wide = residual.astype(jnp.float32)
    ffn_in = (
        residual_wide
        * inverse_rms(jnp.sum(residual_wide * residual_wide, axis=1, keepdims=True), features)
        * ffn_gain.astype(jnp.float32)
    ).astype(jnp.bfloat16)
    pick_count = expert_ids.shape[1]
    local_experts = gate_experts.shape[0]
    experts_total = local_experts * ep_count
    capacity = max(2, (2 * pick_count * sequences + experts_total - 1) // experts_total)
    flat_ids = expert_ids.reshape(-1)
    choose = (flat_ids[:, None] == lax.broadcasted_iota(jnp.int32, (1, experts_total), 1)).astype(
        jnp.int32
    )
    earlier = jnp.cumsum(choose, axis=0) - choose
    slot_of = jnp.sum(earlier * choose, axis=1)
    target = (flat_ids * capacity + slot_of).reshape(sequences, pick_count)
    slot_iota = lax.broadcasted_iota(jnp.int32, (experts_total * capacity, 1, 1), 0)
    placing = jnp.any(slot_iota == target[None, :, :], axis=2).astype(jnp.bfloat16)
    outgoing = jnp.dot(placing, ffn_in, preferred_element_type=jnp.float32).astype(jnp.bfloat16)
    outgoing = outgoing.reshape(ep_count, local_experts, capacity, features)
    arrived = lax.all_to_all(outgoing, "ep", split_axis=0, concat_axis=0, tiled=True)
    gate_act = jnp.einsum(
        "nlcd,ldf->nlcf", arrived, gate_experts, preferred_element_type=jnp.float32
    )
    up_act = jnp.einsum("nlcd,ldf->nlcf", arrived, up_experts, preferred_element_type=jnp.float32)
    active = (jax.nn.silu(gate_act) * up_act).astype(jnp.bfloat16)
    partial_out = jnp.einsum(
        "nlcf,lfd->nlcd", active, down_experts, preferred_element_type=jnp.float32
    )
    summed = lax.psum_scatter(partial_out, "tp", scatter_dimension=3, tiled=True).astype(
        jnp.bfloat16
    )
    returned = lax.all_to_all(summed, "ep", split_axis=0, concat_axis=0, tiled=True)
    result_table = returned.reshape(experts_total * capacity, slice_width)
    selector = (
        target.reshape(-1)[:, None]
        == lax.broadcasted_iota(jnp.int32, (1, experts_total * capacity), 1)
    ).astype(jnp.bfloat16)
    picked = jnp.dot(selector, result_table, preferred_element_type=jnp.float32)
    picked = picked.reshape(sequences, pick_count, slice_width)
    route_weight = jax.nn.softmax(route_logits, axis=1)
    combined = jnp.sum(route_weight[:, :, None] * picked, axis=1)
    squares = lax.psum(jnp.sum(combined * combined, axis=1), "tp")
    own_residual = lax.dynamic_slice_in_dim(residual_wide, tp_place * slice_width, slice_width, 1)
    result = own_residual + combined * inverse_rms(squares, features)[:, None] * out_gain.astype(
        jnp.float32
    )
    return result.astype(jnp.bfloat16)


def solution(mesh):
    placed = (
        P("ep", None),
        P(),
        P("ep", "tp"),
        P("ep", "tp", None),
        P("ep", "tp", None),
        P("ep"),
        P("tp"),
        P("tp", "ep"),
        P(),
        P(),
        P("ep", None),
        P("ep", None),
        P("ep", None, "tp"),
        P("ep", None, "tp"),
        P("ep", "tp", None),
        P("tp"),
    )
    return jax.shard_map(
        per_device, mesh=mesh, in_specs=placed, out_specs=P("ep", "tp"), check_vma=False
    )
```

profile of v0, /device:TPU:0, one launch (start us, length us, event | category | flops | bytes accessed | tf_op | source)
XLA Modules:
  0.0 194.4 jit_solution(17033841998764324074)
XLA Ops:
  6.5 0.7 all-gather.3.cloned.1.call-update
  7.3 0.7 all-gather.5.cloned.1.call-update
  8.1 1.0 fusion.41
  9.0 0.8 copy.51
  10.4 0.7 multiply_add_fusion
  11.2 0.7 convert_element_type.60
  11.8 0.7 convert_element_type.67
  12.5 0.7 convert_element_type.71
  13.2 20.8 %all-gather.3.cloned.1.call-done = bf16[2048,256]{1,0:T(8,128)(2,1)} async-done(((bf16[256,256]{1,0:T(8,128)(2,1)}), bf16[2048,256]{1,0:T(8,128)(2,1)}) %all-gather.3.cloned.1.call-update) | async-done | bytes 1048592 | tf_op jit(solution)/shard_map/all_gather | solution.py:65
  34.0 1.5 convolution_convert_fusion.1
  35.6 3.7 %fusion.67 = f32[12,4,1,1024]{3,2,1,0:T(1,128)S(1)} fusion(bf16[12,4,64,1]{2,3,1,0:T(2,128)(2,1)S(1)} %reshape.143, bf16[12,4,64,1024]{3,2,1,0:T(8,128)(2,1)} %bitcast.94), kind=kOutput, calls=%fused_computation.78 | convolution fusion | flops 6291456 | bytes 6494208 | tf_op jit(solution)/shard_map/she,shec->shc/dot_general | solution.py:16
  39.8 59.4 %reduce-window.6 = f32[12,4,8,128]{3,2,1,0:T(8,128)S(1)} reduce-window(f32[12,4,8,128]{3,2,1,0:T(8,128)S(1)} %reshape.123, f32[]{:T(128)} %constant.13.clone.1), window={size=1x1x1x128 pad=0_0x0_0x0_0x0_127}, to_apply=%region_1.2 | reduce-window | flops 6242304 | bytes 393220 | tf_op jit(solution)/shard_map/reduce-window
  100.6 4.5 %fusion.34 = f32[12,4,1,64]{3,2,1,0:T(1,128)S(1)} fusion(bf16[12,4,64,1024]{3,2,1,0:T(8,128)(2,1)} %bitcast.99, bf16[12,4,1024,1]{2,1,0,3:T(4,128)(2,1)S(1)} %fusion.50), kind=kOutput, calls=%fused_computation.28 | convolution fusion | flops 6291456 | bytes 6402048 | tf_op jit(solution)/shard_map/shc,shec->she/dot_general | solution.py:25
  105.2 1.5 fusion.68
  106.7 18.4 %psum.14 = bf16[12,2048]{1,0:T(8,128)(2,1)S(1)} all-reduce(f32[12,2048]{1,0:T(8,128)S(1)} %fusion.68), channel_id=1, replica_groups=mesh['ep'=8,'tp'=4] {'tp'}, use_global_device_ids=true, to_apply=%region_3.4 | all-reduce | flops 24576 | bytes 147456 | tf_op jit(solution)/shard_map/psum | solution.py:78
  125.8 12.7 %all_to_all.10 = bf16[8,1,6,2048]{3,2,1,0:T(8,128)(2,1)S(1)} all-to-all(bf16[8,1,6,2048]{3,2,1,0:T(8,128)(2,1)S(1)} %bitcast.96), channel_id=1, replica_groups=mesh['ep'=8,'tp'=4] {'ep'}, dimensions={0} | all-to-all | bytes 393216 | tf_op jit(solution)/shard_map/all_to_all | solution.py:107
  138.6 2.0 %fusion.5 = f32[8,1,6,512]{3,0,2,1:T(8,128)S(1)} fusion(bf16[1,2048,512]{2,1,0:T(8,128)(2,1)} %param.28, bf16[8,1,6,2048]{3,2,1,0:T(8,128)(2,1)S(1)} %all_to_all.10), kind=kOutput, calls=%fused_computation.7 | convolution fusion | flops 100663296 | bytes 2392064 | tf_op jit(solution)/shard_map/nlcd,ldf->nlcf/dot_general | solution.py:108
  140.6 3.2 %convolution_bitcast_fusion = f32[8,1,6,2048]{3,0,2,1:T(8,128)} fusion(bf16[1,512,2048]{2,1,0:T(8,128)(2,1)S(1)} %copy-done, bf16[1,2048,512]{2,1,0:T(8,128)(2,1)} %param.29, bf16[8,1,6,2048]{3,2,1,0:T(8,128)(2,1)S(1)} %all_to_all.10, f32[8,1,6,512]{3,0,2,1:T(8,128)S(1)} %fusion.5), kind=kOutput, calls=%fused_computation | convolution fusion | flops 201474048 | bytes 4882432 | tf_op jit(solution)/shard_map/nlcf,lfd->nlcd/dot_general | solution.py:113
  143.8 22.0 %reduce-scatter.2.cloned.1.call-done = f32[8,1,6,512]{3,0,2,1:T(8,128)} async-done(((f32[8,1,6,2048]{3,0,2,1:T(8,128)}), f32[8,1,6,512]{3,0,2,1:T(8,128)}) %reduce-scatter.2.cloned.1.call-update) | async-done | bytes 98320 | tf_op jit(solution)/shard_map/reduce_scatter | solution.py:116
  165.9 0.9 convert_element_type.75
  167.4 4.6 %all-to-all-start.1 = ((bf16[8,1,6,512]{3,2,1,0:T(8,128)(2,1)}), bf16[8,1,6,512]{3,2,1,0:T(8,128)(2,1)S(1)}, u32[]{:S(2)}, u32[]{:S(2)}) async-start(bf16[8,1,6,512]{3,2,1,0:T(8,128)(2,1)} %copy.55), calls=%async_computation.2 | async-start | bytes 131072 | tf_op jit(solution)/shard_map/all_to_all | solution.py:119
  172.1 5.9 %all-to-all-done.1 = bf16[8,1,6,512]{3,2,1,0:T(8,128)(2,1)S(1)} async-done(((bf16[8,1,6,512]{3,2,1,0:T(8,128)(2,1)}), bf16[8,1,6,512]{3,2,1,0:T(8,128)(2,1)S(1)}, u32[]{:S(2)}, u32[]{:S(2)}) %all-to-all-start.1) | async-done | bytes 49184 | tf_op jit(solution)/shard_map/all_to_all | solution.py:119
  178.3 8.9 %psum.15 = f32[12]{0:T(128)S(1)} all-reduce(f32[12]{0:T(128)S(1)} %multiply_reduce_fusion.1), channel_id=1, replica_groups=mesh['ep'=8,'tp'=4] {'tp'}, use_global_device_ids=true, to_apply=%region_14.15 | all-reduce | flops 12 | bytes 96 | tf_op jit(solution)/shard_map/psum | solution.py:129
  187.2 0.7 add_convert_fusion
  (52 shorter events, 4.4 us)
Async XLA Ops:
  6.5 134.0 %copy-start = (bf16[1,512,2048]{2,1,0:T(8,128)(2,1)S(1)}, bf16[1,512,2048]{2,1,0:T(8,128)(2,1)}, u32[]{:S(2)}) copy-start(bf16[1,512,2048]{2,1,0:T(8,128)(2,1)} %param.30) | copy-start | bytes 6291460
  6.5 27.4 %all-gather.3.cloned.1.call-start = ((), (), s32[]{:S(2)}) async-start(), calls=%async_computation.3 | async-start | bytes 1179648 | tf_op jit(solution)/shard_map/all_gather | solution.py:65
  7.3 97.9 %all-gather.5.cloned.1.call-start = ((), (), s32[]{:S(2)}) async-start(), calls=%async_computation.4 | async-start | bytes 1179648 | tf_op jit(solution)/shard_map/all_gather | solution.py:75
  8.0 157.9 %reduce-scatter.2.cloned.1.call-start = ((), (), s32[]{:S(2)}) async-start(), calls=%async_computation.5 | async-start | bytes 491520 | tf_op jit(solution)/shard_map/reduce_scatter | solution.py:116
  35.6 3.8 %copy-start.3 = (f32[4]{0:T(128)S(1)}, f32[4]{0:T(128)}, u32[]{:S(2)}) copy-start(f32[4]{0:T(128)} %param.22) | copy-start | bytes 52
  35.6 3.8 %copy-start.4 = (s32[12]{0:T(128)S(1)}, s32[12]{0:T(128)}, u32[]{:S(2)}) copy-start(s32[12]{0:T(128)} %param.21) | copy-start | bytes 148
  100.5 24.7 %copy-start.1 = (bf16[12,2048]{1,0:T(8,128)(2,1)S(1)}, bf16[12,2048]{1,0:T(8,128)(2,1)}, u32[]{:S(2)}) copy-start(bf16[12,2048]{1,0:T(8,128)(2,1)} %param.16) | copy-start | bytes 147460
  140.6 3.2 %copy-start.2 = (f32[12,2]{0,1:T(2,128)S(1)}, f32[12,2]{0,1:T(2,128)}, u32[]{:S(2)}) copy-start(f32[12,2]{0,1:T(2,128)} %param.27) | copy-start | bytes 292
  140.6 31.5 %copy-start.5 = (bf16[512]{0:T(512)(128)(2,1)S(1)}, bf16[512]{0:T(512)(128)(2,1)}, u32[]{:S(2)}) copy-start(bf16[512]{0:T(512)(128)(2,1)} %param.31) | copy-start | bytes 3076
  167.4 10.5 %all-to-all-start.1 = ((bf16[8,1,6,512]{3,2,1,0:T(8,128)(2,1)}), bf16[8,1,6,512]{3,2,1,0:T(8,128)(2,1)S(1)}, u32[]{:S(2)}, u32[]{:S(2)}) async-start(bf16[8,1,6,512]{3,2,1,0:T(8,128)(2,1)} %copy.55), calls=%async_computation.2 | async-start | bytes 131072 | tf_op jit(solution)/shard_map/all_to_all | solution.py:119
Sparse Core Ops, SparseCore 0:
  8.9 25.0 all-gather.2
  35.6 23.5 all-gather.4
  143.9 21.9 reduce-scatter.1
where the time goes:
time: 195 us; the launch traced here: 194 us
  other arithmetic  66.8 us (34%)
  waiting for transfers between devices  50.1 us (26%)
  blocking collectives  40.1 us (21%)
  matrix products  16.9 us (9%)
  between operations  13.3 us (7%)
  starting transfers between devices  4.69 us (2%)
  local copies, waits for them, and re-layouts  2.53 us (1%)
    another operation x2, other arithmetic  59.5 us
    reduce_scatter x1, waiting for transfers between devices, per_device(): lax.psum_scatter(partial_out, 'tp', scatter_dimension=3, tiled=True)  22 us
    all_gather x1, waiting for transfers between devices, per_device(): lax.all_gather(query_weight, 'ep', axis=0, tiled=True)  20.8 us
    psum x1, blocking collectives, per_device(): attended = lax.psum(partial_value, 'tp').astype(jnp.bfloat16)  18.4 us
    all_to_all x1, blocking collectives, per_device(): lax.all_to_all(outgoing, 'ep', split_axis=0, concat_axis=0, tiled=True)  12.7 us
    psum x1, blocking collectives, per_device(): squares = lax.psum(jnp.sum(combined * combined, axis=1), 'tp')  8.93 us
    all_to_all x1, waiting for transfers between devices, per_device(): lax.all_to_all(summed, 'ep', split_axis=0, concat_axis=0, tiled=True)  5.88 us
    all_to_all x1, starting transfers between devices, per_device(): lax.all_to_all(summed, 'ep', split_axis=0, concat_axis=0, tiled=True)  4.61 us
  transfers between devices with their start and end apart: 4, of which 3 were waited for; matrix products, arithmetic and copies ran while one was open for 39% of the time, Pallas kernels for 0%

commit v1 on v0

--- a/solution.py
+++ b/solution.py
@@ -75,7 +75,9 @@
         lax.all_gather(out_weight, "ep", axis=1, tiled=True),
         preferred_element_type=jnp.float32,
     )
-    attended = lax.psum(partial_value, "tp").astype(jnp.bfloat16)
+    attended = jnp.sum(jax.lax.all_gather(partial_value, axis_name="tp"), axis=0).astype(
+        jnp.bfloat16
+    )
     attended = lax.optimization_barrier(attended).astype(jnp.float32)
     residual = (
         hidden_wide

time: 195 us -> 187 us (0.959)
  blocking collectives: 40.1 us -> 31.7 us
    psum x1 -> x0, blocking collectives: 18.4 us -> none  [per_device(): attended = lax.psum(partial_value, 'tp').astype(jnp.bfloat16)]
    all_gather x0 -> x1, blocking collectives: none -> 10 us  [per_device(): jax.lax.all_gather(partial_value, axis_name='tp')]
  transfers between devices with their start and end apart: 4 -> 4, of which waited for: 3 -> 3; matrix products, arithmetic and copies ran while one was open for 39% -> 41% of each run, Pallas kernels for 0% -> 0%
where the time goes in v1:
time: 187 us
  other arithmetic  66.9 us (36%)
  waiting for transfers between devices  50.9 us (27%)
  blocking collectives  31.7 us (17%)
  matrix products  16.9 us (9%)
  between operations  13.3 us (7%)
  starting transfers between devices  4.69 us (3%)
  local copies, waits for them, and re-layouts  2.52 us (1%)
    another operation x2, other arithmetic  59.5 us
    reduce_scatter x1, waiting for transfers between devices, per_device(): lax.psum_scatter(partial_out, 'tp', scatter_dimension=3, tiled=True)  22.8 us
    all_gather x1, waiting for transfers between devices, per_device(): lax.all_gather(query_weight, 'ep', axis=0, tiled=True)  20.8 us
    all_to_all x1, blocking collectives, per_device(): lax.all_to_all(outgoing, 'ep', split_axis=0, concat_axis=0, tiled=True)  12.8 us
    all_gather x1, blocking collectives, per_device(): jax.lax.all_gather(partial_value, axis_name='tp')  10 us
    psum x1, blocking collectives, per_device(): squares = lax.psum(jnp.sum(combined * combined, axis=1), 'tp')  8.92 us
    all_to_all x1, waiting for transfers between devices, per_device(): lax.all_to_all(summed, 'ep', split_axis=0, concat_axis=0, tiled=True)  5.88 us
    all_to_all x1, starting transfers between devices, per_device(): lax.all_to_all(summed, 'ep', split_axis=0, concat_axis=0, tiled=True)  4.61 us
  transfers between devices with their start and end apart: 4, of which 3 were waited for; matrix products, arithmetic and copies ran while one was open for 41% of the time, Pallas kernels for 0%

profile of v1, /device:TPU:0, one launch (start us, length us, event | category | flops | bytes accessed | tf_op | source)
XLA Modules:
  0.0 186.8 jit_solution(9585491430346848270)
XLA Ops:
  6.5 0.7 all-gather.5.cloned.1.call-update
  7.3 0.7 all-gather.7.cloned.1.call-update
  8.1 1.0 fusion.41
  9.0 0.8 copy.51
  10.4 0.7 multiply_add_fusion
  11.2 0.7 convert_element_type.60
  11.8 0.7 convert_element_type.67
  12.5 0.7 convert_element_type.71
  13.2 20.8 %all-gather.5.cloned.1.call-done = bf16[2048,256]{1,0:T(8,128)(2,1)} async-done(((bf16[256,256]{1,0:T(8,128)(2,1)}), bf16[2048,256]{1,0:T(8,128)(2,1)}) %all-gather.5.cloned.1.call-update) | async-done | bytes 1048592 | tf_op jit(solution)/shard_map/all_gather | solution.py:65
  34.0 1.5 convolution_convert_fusion.1
  35.6 3.7 %fusion.67 = f32[12,4,1,1024]{3,2,1,0:T(1,128)S(1)} fusion(bf16[12,4,64,1]{2,3,1,0:T(2,128)(2,1)S(1)} %reshape.147, bf16[12,4,64,1024]{3,2,1,0:T(8,128)(2,1)} %bitcast.96), kind=kOutput, calls=%fused_computation.79 | convolution fusion | flops 6291456 | bytes 6494208 | tf_op jit(solution)/shard_map/she,shec->shc/dot_general | solution.py:16
  39.8 59.4 %reduce-window.6 = f32[12,4,8,128]{3,2,1,0:T(8,128)S(1)} reduce-window(f32[12,4,8,128]{3,2,1,0:T(8,128)S(1)} %reshape.123, f32[]{:T(128)} %constant.13.clone.1), window={size=1x1x1x128 pad=0_0x0_0x0_0x0_127}, to_apply=%region_1.2 | reduce-window | flops 6242304 | bytes 393220 | tf_op jit(solution)/shard_map/reduce-window
  100.5 4.5 %fusion.34 = f32[12,4,1,64]{3,2,1,0:T(1,128)S(1)} fusion(bf16[12,4,64,1024]{3,2,1,0:T(8,128)(2,1)} %bitcast.101, bf16[12,4,1024,1]{2,1,0,3:T(4,128)(2,1)S(1)} %fusion.50), kind=kOutput, calls=%fused_computation.29 | convolution fusion | flops 6291456 | bytes 6402048 | tf_op jit(solution)/shard_map/shc,shec->she/dot_general | solution.py:25
  105.2 1.5 convolution_bitcast_fusion.1
  106.7 10.0 %all-gather.1 = f32[4,12,2048]{2,1,0:T(8,128)S(1)} all-gather(f32[1,12,2048]{2,1,0:T(8,128)S(1)} %convolution_bitcast_fusion.1), channel_id=2, replica_groups=mesh['ep'=8,'tp'=4] {'tp'}, dimensions={0}, use_global_device_ids=true | all-gather | bytes 491520 | tf_op jit(solution)/shard_map/all_gather | solution.py:78
  117.4 12.8 %all_to_all.10 = bf16[8,1,6,2048]{3,2,1,0:T(8,128)(2,1)S(1)} all-to-all(bf16[8,1,6,2048]{3,2,1,0:T(8,128)(2,1)S(1)} %bitcast.98), channel_id=1, replica_groups=mesh['ep'=8,'tp'=4] {'ep'}, dimensions={0} | all-to-all | bytes 393216 | tf_op jit(solution)/shard_map/all_to_all | solution.py:109
  130.2 2.0 %fusion.5 = f32[8,1,6,512]{3,0,2,1:T(8,128)S(1)} fusion(bf16[1,2048,512]{2,1,0:T(8,128)(2,1)} %param.28, bf16[8,1,6,2048]{3,2,1,0:T(8,128)(2,1)S(1)} %all_to_all.10), kind=kOutput, calls=%fused_computation.8 | convolution fusion | flops 100663296 | bytes 2392064 | tf_op jit(solution)/shard_map/nlcd,ldf->nlcf/dot_general | solution.py:110
  132.2 3.2 %convolution_bitcast_fusion = f32[8,1,6,2048]{3,0,2,1:T(8,128)} fusion(bf16[1,512,2048]{2,1,0:T(8,128)(2,1)S(1)} %copy-done, bf16[1,2048,512]{2,1,0:T(8,128)(2,1)} %param.29, bf16[8,1,6,2048]{3,2,1,0:T(8,128)(2,1)S(1)} %all_to_all.10, f32[8,1,6,512]{3,0,2,1:T(8,128)S(1)} %fusion.5), kind=kOutput, calls=%fused_computation | convolution fusion | flops 201474048 | bytes 4882432 | tf_op jit(solution)/shard_map/nlcf,lfd->nlcd/dot_general | solution.py:115
  135.5 22.8 %reduce-scatter.2.cloned.1.call-done = f32[8,1,6,512]{3,0,2,1:T(8,128)} async-done(((f32[8,1,6,2048]{3,0,2,1:T(8,128)}), f32[8,1,6,512]{3,0,2,1:T(8,128)}) %reduce-scatter.2.cloned.1.call-update) | async-done | bytes 98320 | tf_op jit(solution)/shard_map/reduce_scatter | solution.py:118
  158.3 0.9 convert_element_type.75
  159.8 4.6 %all-to-all-start.1 = ((bf16[8,1,6,512]{3,2,1,0:T(8,128)(2,1)}), bf16[8,1,6,512]{3,2,1,0:T(8,128)(2,1)S(1)}, u32[]{:S(2)}, u32[]{:S(2)}) async-start(bf16[8,1,6,512]{3,2,1,0:T(8,128)(2,1)} %copy.55), calls=%async_computation.2 | async-start | bytes 131072 | tf_op jit(solution)/shard_map/all_to_all | solution.py:121
  164.5 5.9 %all-to-all-done.1 = bf16[8,1,6,512]{3,2,1,0:T(8,128)(2,1)S(1)} async-done(((bf16[8,1,6,512]{3,2,1,0:T(8,128)(2,1)}), bf16[8,1,6,512]{3,2,1,0:T(8,128)(2,1)S(1)}, u32[]{:S(2)}, u32[]{:S(2)}) %all-to-all-start.1) | async-done | bytes 49184 | tf_op jit(solution)/shard_map/all_to_all | solution.py:121
  170.7 8.9 %psum.7 = f32[12]{0:T(128)S(1)} all-reduce(f32[12]{0:T(128)S(1)} %multiply_reduce_fusion.1), channel_id=1, replica_groups=mesh['ep'=8,'tp'=4] {'tp'}, use_global_device_ids=true, to_apply=%region_14.15 | all-reduce | flops 12 | bytes 96 | tf_op jit(solution)/shard_map/psum | solution.py:131
  179.6 0.7 add_convert_fusion
  (53 shorter events, 4.4 us)
Async XLA Ops:
  6.5 125.7 %copy-start = (bf16[1,512,2048]{2,1,0:T(8,128)(2,1)S(1)}, bf16[1,512,2048]{2,1,0:T(8,128)(2,1)}, u32[]{:S(2)}) copy-start(bf16[1,512,2048]{2,1,0:T(8,128)(2,1)} %param.30) | copy-start | bytes 6291460
  6.5 27.4 %all-gather.5.cloned.1.call-start = ((), (), s32[]{:S(2)}) async-start(), calls=%async_computation.3 | async-start | bytes 1179648 | tf_op jit(solution)/shard_map/all_gather | solution.py:65
  7.3 97.9 %all-gather.7.cloned.1.call-start = ((), (), s32[]{:S(2)}) async-start(), calls=%async_computation.4 | async-start | bytes 1179648 | tf_op jit(solution)/shard_map/all_gather | solution.py:75
  8.0 150.3 %reduce-scatter.2.cloned.1.call-start = ((), (), s32[]{:S(2)}) async-start(), calls=%async_computation.5 | async-start | bytes 491520 | tf_op jit(solution)/shard_map/reduce_scatter | solution.py:118
  35.6 3.8 %copy-start.3 = (f32[4]{0:T(128)S(1)}, f32[4]{0:T(128)}, u32[]{:S(2)}) copy-start(f32[4]{0:T(128)} %param.22) | copy-start | bytes 52
  35.6 3.8 %copy-start.4 = (s32[12]{0:T(128)S(1)}, s32[12]{0:T(128)}, u32[]{:S(2)}) copy-start(s32[12]{0:T(128)} %param.21) | copy-start | bytes 148
  105.1 11.8 %copy-start.1 = (bf16[12,2048]{1,0:T(8,128)(2,1)S(1)}, bf16[12,2048]{1,0:T(8,128)(2,1)}, u32[]{:S(2)}) copy-start(bf16[12,2048]{1,0:T(8,128)(2,1)} %param.16) | copy-start | bytes 147460
  132.2 3.2 %copy-start.2 = (f32[12,2]{0,1:T(2,128)S(1)}, f32[12,2]{0,1:T(2,128)}, u32[]{:S(2)}) copy-start(f32[12,2]{0,1:T(2,128)} %param.27) | copy-start | bytes 292
  132.2 32.2 %copy-start.5 = (bf16[512]{0:T(512)(128)(2,1)S(1)}, bf16[512]{0:T(512)(128)(2,1)}, u32[]{:S(2)}) copy-start(bf16[512]{0:T(512)(128)(2,1)} %param.31) | copy-start | bytes 3076
  159.8 10.5 %all-to-all-start.1 = ((bf16[8,1,6,512]{3,2,1,0:T(8,128)(2,1)}), bf16[8,1,6,512]{3,2,1,0:T(8,128)(2,1)S(1)}, u32[]{:S(2)}, u32[]{:S(2)}) async-start(bf16[8,1,6,512]{3,2,1,0:T(8,128)(2,1)} %copy.55), calls=%async_computation.2 | async-start | bytes 131072 | tf_op jit(solution)/shard_map/all_to_all | solution.py:121
Sparse Core Ops, SparseCore 0:
  8.9 25.0 all-gather.4
  35.6 23.5 all-gather.6
  135.5 22.6 reduce-scatter.1
